TPU v7x, 32 devices: a whole 2x2x4 slice. The times are simulated.
32 devices in a mesh: sp: 8 (over z, y), tp: 4 (over x, core).
Axes of the slice: x: 2, y: 2, z: 4, core: 2. Of those that a mesh axis runs over, the one named last changes fastest.
Arguments:
- queries: bfloat16 [6144, 1024], P('sp', 'tp'), may hold values from -8 to 8
- keys: bfloat16 [6144, 256], P('sp', 'tp'), may hold values from -8 to 8
- values: bfloat16 [6144, 256], P('sp', 'tp'), may hold values from -18 to 18
- query_gain: float32 [64], replicated, may hold values from 0.4 to 5.5
- key_gain: float32 [64], replicated, may hold values from 0.4 to 5.5
- sink_logits: float32 [16], P('tp'), may hold values from 2 to 5
- out_weight: bfloat16 [1024, 2048], P('tp'), may hold values from -0.1875 to 0.1875
- residual: bfloat16 [6144, 2048], P('sp', 'tp'), may hold values from -21 to 21
- norm_gain: float32 [2048], P('tp'), may hold values from 0.1 to 1.9
- gate_weight: bfloat16 [2048, 5632], P('sp', 'tp'), may hold values from -0.125 to 0.125
- up_weight: bfloat16 [2048, 5632], P('sp', 'tp'), may hold values from -0.125 to 0.125
- down_weight: bfloat16 [5632, 2048], P('tp', 'sp'), may hold values from -0.078125 to 0.078125
Outputs:
- layer_out: bfloat16 [6144, 2048], P('sp', 'tp')
All inputs are finite; a program needn't handle non-finite values.
Results may differ from a plain program's by a relative error of at most 0.0095.
The roundings to bfloat16 on the way count: a program that leaves them out, or rounds other values in their place, can miss the bound.
Values may be sent and summed in bfloat16 or wider, within the bound.
No kernel may reach another device: no remote copies, remote signals or barrier semaphores. Data moves between devices by JAX's collectives and lax.ppermute only.
A program may use at most 192 MiB of HBM per device.

v0:
```python
import jax
import jax.numpy as jnp
from jax import lax
from jax.sharding import PartitionSpec as P

D = 2048
WINDOW = 128


def from_behind(block, axis, distance):
    devices = range(lax.axis_size(axis))
    route = [(i - distance, i) for i in devices if i - distance in devices]
    return lax.ppermute(block, axis, route)


def norm_heads(flat, gain, heads):
    row_count = flat.shape[0]
    head_width = gain.shape[0]
    data = flat.astype(jnp.float32).reshape(row_count, heads, head_width)
    scaled = data * lax.rsqrt(jnp.mean(data * data, axis=-1, keepdims=True) + 1e-06) * gain
    return scaled.astype(jnp.bfloat16)


def per_device(
    queries,
    keys,
    values,
    query_gain,
    key_gain,
    sink_logits,
    out_weight,
    residual,
    norm_gain,
    gate_weight,
    up_weight,
    down_weight,
):
    head_width = query_gain.shape[0]
    row_count = queries.shape[0]
    q_heads = queries.shape[1] // head_width
    k_heads = keys.shape[1] // head_width
    group_size = q_heads // k_heads
    window_len = WINDOW
    block_count = row_count // window_len
    gate_full, up_full = (
        lax.all_gather(gate_weight, "sp", axis=0, tiled=True),
        lax.all_gather(up_weight, "sp", axis=0, tiled=True),
    )
    down_full = lax.all_gather(down_weight, "sp", axis=1, tiled=True)
    query_norm = norm_heads(queries, query_gain, q_heads)
    key_norm = norm_heads(keys, key_gain, k_heads).reshape(row_count, k_heads * head_width)
    prev_keys, prev_values = from_behind(
        (key_norm[row_count - window_len :], values[row_count - window_len :]), "sp", 1
    )
    key_all = jnp.concatenate([prev_keys, key_norm], axis=0)
    value_all = jnp.concatenate([prev_values, values], axis=0)
    key_blocks = jnp.concatenate(
        [
            key_all[:row_count].reshape(block_count, window_len, k_heads, head_width),
            key_norm.reshape(block_count, window_len, k_heads, head_width),
        ],
        axis=1,
    )
    value_blocks = jnp.concatenate(
        [
            value_all[:row_count].reshape(block_count, window_len, k_heads, head_width),
            values.reshape(block_count, window_len, k_heads, head_width),
        ],
        axis=1,
    )
    query_blocks = query_norm.reshape(block_count, window_len, k_heads, group_size, head_width)
    scores = jnp.einsum(
        "nqhgd,nkhd->nhgqk", query_blocks, key_blocks, preferred_element_type=jnp.float32
    ) * head_width ** (-0.5)
    query_index = jnp.arange(window_len)[:, None]
    key_index = jnp.arange(2 * window_len)[None, :]
    offset_lag = window_len + query_index - key_index
    inband = (offset_lag >= 0) & (offset_lag < window_len)
    leading = (
        (jnp.arange(block_count)[:, None, None] > 0)
        | (key_index[None] >= window_len)
        | (lax.axis_index("sp") > 0)
    )
    valid = inband[None] & leading
    scores = jnp.where(valid[:, None, None], scores, -1e30)
    sink_rows = sink_logits.reshape(k_heads, group_size)[None, :, :, None]
    row_peak = jnp.maximum(jnp.max(scores, axis=-1), sink_rows)
    exp_terms = jnp.exp(scores - row_peak[..., None])
    denom_sum = jnp.sum(exp_terms, axis=-1) + jnp.exp(sink_rows - row_peak)
    weights = (exp_terms / denom_sum[..., None]).astype(jnp.bfloat16)
    attended = jnp.einsum(
        "nhgqk,nkhd->nqhgd", weights, value_blocks, preferred_element_type=jnp.float32
    ).astype(jnp.bfloat16)
    attended = attended.reshape(row_count, q_heads * head_width)
    projected = jnp.dot(attended, out_weight, preferred_element_type=jnp.float32)
    mixed = lax.psum_scatter(
        projected.astype(jnp.bfloat16), "tp", scatter_dimension=1, tiled=True
    ).astype(jnp.float32)
    middle_wide = (residual.astype(jnp.float32) + mixed).astype(jnp.bfloat16).astype(jnp.float32)
    squares = lax.psum(jnp.sum(middle_wide * middle_wide, axis=1), "tp")
    normed = (middle_wide * lax.rsqrt(squares / D + 1e-06)[:, None] * norm_gain).astype(
        jnp.bfloat16
    )
    normed_all = lax.all_gather(normed, "tp", axis=1, tiled=True)
    gate_acts = jnp.dot(normed_all, gate_full, preferred_element_type=jnp.float32)
    up_acts = jnp.dot(normed_all, up_full, preferred_element_type=jnp.float32)
    hidden = (jax.nn.silu(gate_acts) * up_acts).astype(jnp.bfloat16)
    down_terms = jnp.dot(hidden, down_full, preferred_element_type=jnp.float32)
    summed_back = lax.psum_scatter(
        down_terms.astype(jnp.bfloat16), "tp", scatter_dimension=1, tiled=True
    ).astype(jnp.float32)
    return (middle_wide + 0.5 * summed_back).astype(jnp.bfloat16)


def solution(mesh):
    in_specs = (
        P("sp", "tp"),
        P("sp", "tp"),
        P("sp", "tp"),
        P(),
        P(),
        P("tp"),
        P("tp", None),
        P("sp", "tp"),
        P("tp"),
        P("sp", "tp"),
        P("sp", "tp"),
        P("tp", "sp"),
    )
    out_specs = P("sp", "tp")
    return jax.shard_map(
        per_device, mesh=mesh, in_specs=in_specs, out_specs=out_specs, check_vma=False
    )
```

profile of v0, /device:TPU:0, one launch (start us, length us, event | category | flops | bytes accessed | tf_op | source)
XLA Modules:
  0.0 404.4 jit_solution(5352290155806493148)
XLA Ops:
  7.4 1.0 fusion.19
  8.4 1.0 fusion.21
  9.4 4.9 %collective-permute-start.1 = (bf16[128,64]{0,1:T(8,128)(2,1)S(1)}, bf16[128,64]{0,1:T(8,128)(2,1)S(1)}, u32[]{:S(2)}, u32[]{:S(2)}) collective-permute-start(bf16[128,64]{0,1:T(8,128)(2,1)S(1)} %slice.18), channel_id=1, source_target_pairs={{0,4},{4,8},{8,12},{12,16},{16,20},{20,24},{24,28},{1,5},{5,9},{9,... | collective-permute-start | bytes 49160 | tf_op jit(solution)/shard_map/ppermute | solution.py:13
  14.3 0.7 slice.14
  15.0 3.4 collective-permute-start
  18.5 1.2 copy.19
  19.6 0.4 reshape.185
  20.3 0.8 multiply_convert_fusion.1
  21.2 0.3 broadcast_and_fusion
  21.5 0.1 reshape_reshape.3
  22.0 0.6 fusion.1
  22.8 1.6 copy-done.3
  24.3 0.7 fusion
  25.3 2.8 fusion.12
  28.2 0.3 copy.22
  28.4 2.7 convolution_convert_fusion
  31.3 0.5 all-gather.7.cloned.1.call-update
  31.8 37.5 %reduce-scatter.3.cloned.1.call-done = bf16[768,512]{1,0:T(8,128)(2,1)} async-done(((bf16[768,2048]{1,0:T(8,128)(2,1)}), bf16[768,512]{1,0:T(8,128)(2,1)}) %reduce-scatter.3.cloned.1.call-update) | async-done | bytes 786448 | tf_op jit(solution)/shard_map/reduce_scatter | solution.py:96
  69.3 1.5 fusion.2
  70.8 5.8 %psum.7 = f32[768]{0:T(1024)S(1)} all-reduce(f32[768]{0:T(1024)S(1)} %fusion.2), channel_id=1, replica_groups=mesh['sp'=8,'tp'=4] {'tp'}, use_global_device_ids=true, to_apply=%region_6.7 | all-reduce | flops 768 | bytes 6144 | tf_op jit(solution)/shard_map/psum | solution.py:100
  76.5 2.3 fusion.4
  78.9 0.5 all-gather.11.cloned.1.call-update
  79.5 0.7 all-gather.9.cloned.1.call-update
  80.2 0.2 reduce-scatter.5.cloned.1.call-start
  80.4 45.8 %all-gather.7.cloned.1.call-done = bf16[2048,1408]{1,0:T(8,128)(2,1)} async-done(((bf16[256,1408]{1,0:T(8,128)(2,1)}), bf16[2048,1408]{1,0:T(8,128)(2,1)}) %all-gather.7.cloned.1.call-update) | async-done | bytes 5767184 | tf_op jit(solution)/shard_map/all_gather | solution.py:46
  126.3 28.0 %all-gather.5.cloned.1.call-done = bf16[768,2048]{1,0:T(8,128)(2,1)} async-done(((bf16[768,512]{1,0:T(8,128)(2,1)}), bf16[768,2048]{1,0:T(8,128)(2,1)}) %all-gather.5.cloned.1.call-update) | async-done | bytes 3145744 | tf_op jit(solution)/shard_map/all_gather | solution.py:104
  154.3 9.7 %fusion.34 = f32[768,1408]{1,0:T(8,128)} fusion(bf16[768,2048]{1,0:T(8,128)(2,1)} %all-gather.5.cloned.1.call-done, bf16[2048,1408]{1,0:T(8,128)(2,1)} %all-gather.7.cloned.1.call-done), kind=kOutput, calls=%fused_computation.60 | convolution fusion | flops 4429185024 | bytes 13238272 | tf_op jit(solution)/shard_map/dot_general | solution.py:105
  163.9 85.2 %all-gather.11.cloned.1.call-done = bf16[1408,2048]{1,0:T(8,128)(2,1)} async-done(((bf16[1408,256]{1,0:T(8,128)(2,1)}), bf16[1408,2048]{1,0:T(8,128)(2,1)}) %all-gather.11.cloned.1.call-update) | async-done | bytes 5767184 | tf_op jit(solution)/shard_map/all_gather | solution.py:49
  249.1 92.5 %all-gather.9.cloned.1.call-done = bf16[2048,1408]{1,0:T(8,128)(2,1)} async-done(((bf16[256,1408]{1,0:T(8,128)(2,1)}), bf16[2048,1408]{1,0:T(8,128)(2,1)}) %all-gather.9.cloned.1.call-update) | async-done | bytes 5767184 | tf_op jit(solution)/shard_map/all_gather | solution.py:47
  341.6 16.8 %convolution_convert_fusion.1 = bf16[768,2048]{1,0:T(8,128)(2,1)} fusion(bf16[1408,2048]{1,0:T(8,128)(2,1)} %all-gather.11.cloned.1.call-done, f32[768,1408]{1,0:T(8,128)} %fusion.34, bf16[768,2048]{1,0:T(8,128)(2,1)} %all-gather.5.cloned.1.call-done, bf16[2048,1408]{1,0:T(8,128)(2,1)} %all-gather.9.cloned.1.call-done), kind=kOutput, calls=%fused_computation.2 | convolution fusion | flops 8866430976 | bytes 22151168 | tf_op jit(solution)/shard_map/dot_general | solution.py:108
  358.4 36.0 %reduce-scatter.5.cloned.1.call-done = bf16[768,512]{1,0:T(8,128)(2,1)} async-done(((bf16[768,2048]{1,0:T(8,128)(2,1)}), bf16[768,512]{1,0:T(8,128)(2,1)}) %reduce-scatter.5.cloned.1.call-update) | async-done | bytes 786448 | tf_op jit(solution)/shard_map/reduce_scatter | solution.py:109
  394.5 2.3 fusion.5
  (45 shorter events, 1.2 us)
Async XLA Ops:
  7.4 21.1 %copy-start = (bf16[256,2048]{1,0:T(8,128)(2,1)S(1)}, bf16[256,2048]{1,0:T(8,128)(2,1)}, u32[]{:S(2)}) copy-start(bf16[256,2048]{1,0:T(8,128)(2,1)} %param.18) | copy-start | bytes 3145732
  7.4 14.3 %copy-start.4 = (bf16[768,64]{0,1:T(8,128)(2,1)S(1)}, bf16[768,64]{0,1:T(8,128)(2,1)}, u32[]{:S(2)}) copy-start(bf16[768,64]{0,1:T(8,128)(2,1)} %param.14) | copy-start | bytes 294916
  7.4 61.9 %reduce-scatter.3.cloned.1.call-start = ((), (), s32[]{:S(2)}) async-start(), calls=%async_computation.2 | async-start | bytes 3932160 | tf_op jit(solution)/shard_map/reduce_scatter | solution.py:96
  9.4 12.4 %collective-permute-start.1 = (bf16[128,64]{0,1:T(8,128)(2,1)S(1)}, bf16[128,64]{0,1:T(8,128)(2,1)S(1)}, u32[]{:S(2)}, u32[]{:S(2)}) collective-permute-start(bf16[128,64]{0,1:T(8,128)(2,1)S(1)} %slice.18), channel_id=1, source_target_pairs={{0,4},{4,8},{8,12},{12,16},{16,20},{20,24},{24,28},{1,5},{5,9},{9,... | collective-permute-start | bytes 49160 | tf_op jit(solution)/shard_map/ppermute | solution.py:13
  15.0 10.1 %collective-permute-start = (bf16[128,64]{0,1:T(8,128)(2,1)S(1)}, bf16[128,64]{0,1:T(8,128)(2,1)S(1)}, u32[]{:S(2)}, u32[]{:S(2)}) collective-permute-start(bf16[128,64]{0,1:T(8,128)(2,1)S(1)} %slice.14), channel_id=1, source_target_pairs={{0,4},{4,8},{8,12},{12,16},{16,20},{20,24},{24,28},{1,5},{5,9},{9,... | collective-permute-start | bytes 49160 | tf_op jit(solution)/shard_map/ppermute | solution.py:13
  21.1 1.6 copy-start.5
  22.7 1.6 copy-start.3
  31.2 38.1 %copy-start.1 = (bf16[768,512]{1,0:T(8,128)(2,1)S(1)}, bf16[768,512]{1,0:T(8,128)(2,1)}, u32[]{:S(2)}) copy-start(bf16[768,512]{1,0:T(8,128)(2,1)} %param.19) | copy-start | bytes 2359300
  31.2 45.4 %copy-start.6 = (f32[512]{0:T(512)S(1)}, f32[512]{0:T(512)}, u32[]{:S(2)}) copy-start(f32[512]{0:T(512)} %param.20) | copy-start | bytes 6148
  31.2 95.1 %all-gather.7.cloned.1.call-start = ((), (), s32[]{:S(2)}) async-start(), calls=%async_computation.4 | async-start | bytes 6488064 | tf_op jit(solution)/shard_map/all_gather | solution.py:46
  31.8 122.5 %all-gather.5.cloned.1.call-start = ((), (), s32[]{:S(2)}) async-start(), calls=%async_computation.3 | async-start | bytes 3932160 | tf_op jit(solution)/shard_map/all_gather | solution.py:104
  78.9 170.2 %all-gather.11.cloned.1.call-start = ((), (), s32[]{:S(2)}) async-start(), calls=%async_computation.6 | async-start | bytes 6488064 | tf_op jit(solution)/shard_map/all_gather | solution.py:49
  79.5 262.2 %all-gather.9.cloned.1.call-start = ((), (), s32[]{:S(2)}) async-start(), calls=%async_computation.5 | async-start | bytes 6488064 | tf_op jit(solution)/shard_map/all_gather | solution.py:47
  80.2 314.3 %reduce-scatter.5.cloned.1.call-start = ((), (), s32[]{:S(2)}) async-start(), calls=%async_computation.7 | async-start | bytes 3932160 | tf_op jit(solution)/shard_map/reduce_scatter | solution.py:109
  358.4 36.1 %copy-start.2 = (bf16[768,512]{1,0:T(8,128)(2,1)S(1)}, bf16[768,512]{1,0:T(8,128)(2,1)}, u32[]{:S(2)}) copy-start(bf16[768,512]{1,0:T(8,128)(2,1)} %reduce-scatter.3.cloned.1.call-done) | copy-start | bytes 2359300
Sparse Core Ops, SparseCore 0:
  31.3 37.9 reduce-scatter.2
  358.6 35.8 reduce-scatter.4
Sparse Core Ops, SparseCore 1:
  33.9 92.3 all-gather.6
  127.7 26.5 all-gather.4
  156.2 92.9 all-gather.10
  251.3 90.3 all-gather.8
where the time goes:
time: 405 us; the launch traced here: 404 us
  waiting for transfers between devices  327 us (81%)
  matrix products  32.7 us (8%)
  between operations  15.3 us (4%)
  other arithmetic  10.4 us (3%)
  starting transfers between devices  8.71 us (2%)
  blocking collectives  5.77 us (1%)
  local copies, waits for them, and re-layouts  4.77 us (1%)
    all_gather x1, waiting for transfers between devices, per_device(): lax.all_gather(up_weight, 'sp', axis=0, tiled=True)  92.5 us
    all_gather x1, waiting for transfers between devices, per_device(): down_full = lax.all_gather(down_weight, 'sp', axis=1, tiled=True)  85.2 us
    all_gather x1, waiting for transfers between devices, per_device(): lax.all_gather(gate_weight, 'sp', axis=0, tiled=True)  45.8 us
    reduce_scatter x1, waiting for transfers between devices, per_device(): lax.psum_scatter(projected.astype(jnp.bfloat16), 'tp', scatter_dimension=...  37.5 us
    reduce_scatter x1, waiting for transfers between devices, per_device(): lax.psum_scatter(down_terms.astype(jnp.bfloat16), 'tp', scatter_dimension...  36 us
    all_gather x1, waiting for transfers between devices, per_device(): normed_all = lax.all_gather(normed, 'tp', axis=1, tiled=True)  28 us
    dot_general x1, matrix products, per_device(): down_terms = jnp.dot(hidden, down_full, preferred_element_type=jnp.float32)  16.8 us
    dot_general x1, matrix products, per_device(): jnp.dot(normed_all, gate_full, preferred_element_type=jnp.float32)  9.67 us
  transfers between devices with their start and end apart: 8, of which 6 were waited for; matrix products, arithmetic and copies ran while one was open for 5% of the time, Pallas kernels for 0%

commit v1 on v0

--- a/solution.py
+++ b/solution.py
@@ -44,7 +44,9 @@
     block_count = row_count // window_len
     gate_full, up_full = (
         lax.all_gather(gate_weight, "sp", axis=0, tiled=True),
-        lax.all_gather(up_weight, "sp", axis=0, tiled=True),
+        jnp.concatenate(
+            lax.all_to_all(jnp.stack([up_weight] * lax.axis_size("sp")), "sp", 0, 0), axis=0
+        ),
     )
     down_full = lax.all_gather(down_weight, "sp", axis=1, tiled=True)
     query_norm = norm_heads(queries, query_gain, q_heads)

time: 405 us -> 392 us (0.968)
  waiting for transfers between devices: 327 us -> 305 us
  starting transfers between devices: 8.71 us -> 14.4 us
    all_gather x1 -> x0, waiting for transfers between devices: 92.5 us -> none  [per_device(): lax.all_gather(up_weight, 'sp', axis=0, tiled=True)]
    all_gather x1, waiting for transfers between devices: 45.8 us -> 83.8 us  [per_device(): lax.all_gather(gate_weight, 'sp', axis=0, tiled=True)]
    all_gather x1, waiting for transfers between devices: 28 us -> 54.1 us  [per_device(): normed_all = lax.all_gather(normed, 'tp', axis=1, tiled=True)]
    all_to_all x0 -> x1, waiting for transfers between devices: none -> 26.1 us  [per_device(): lax.all_to_all(jnp.stack([up_weight] * lax.axis_size('sp')), 'sp', 0, 0)]
    all_gather x1, waiting for transfers between devices: 85.2 us -> 66.4 us  [per_device(): down_full = lax.all_gather(down_weight, 'sp', axis=1, tiled=True)]
    all_to_all x0 -> x1, starting transfers between devices: none -> 5.71 us  [per_device(): lax.all_to_all(jnp.stack([up_weight] * lax.axis_size('sp')), 'sp', 0, 0)]
  transfers between devices with their start and end apart: 8 -> 8, of which waited for: 6 -> 6; matrix products, arithmetic and copies ran while one was open for 5% -> 6% of each run, Pallas kernels for 0% -> 0%
where the time goes in v1:
time: 392 us; the launch traced here: 391 us
  waiting for transfers between devices  305 us (78%)
  matrix products  32.7 us (8%)
  between operations  15.3 us (4%)
  starting transfers between devices  14.4 us (4%)
  other arithmetic  10.4 us (3%)
  local copies, waits for them, and re-layouts  7.69 us (2%)
  blocking collectives  5.77 us (1%)
    all_gather x1, waiting for transfers between devices, per_device(): lax.all_gather(gate_weight, 'sp', axis=0, tiled=True)  83.8 us
    all_gather x1, waiting for transfers between devices, per_device(): down_full = lax.all_gather(down_weight, 'sp', axis=1, tiled=True)  66.4 us
    all_gather x1, waiting for transfers between devices, per_device(): normed_all = lax.all_gather(normed, 'tp', axis=1, tiled=True)  54.1 us
    reduce_scatter x1, waiting for transfers between devices, per_device(): lax.psum_scatter(projected.astype(jnp.bfloat16), 'tp', scatter_dimension=...  37.5 us
    reduce_scatter x1, waiting for transfers between devices, per_device(): lax.psum_scatter(down_terms.astype(jnp.bfloat16), 'tp', scatter_dimension...  36.1 us
    all_to_all x1, waiting for transfers between devices, per_device(): lax.all_to_all(jnp.stack([up_weight] * lax.axis_size('sp')), 'sp', 0, 0)  26.1 us
    dot_general x1, matrix products, per_device(): down_terms = jnp.dot(hidden, down_full, preferred_element_type=jnp.float32)  16.9 us
    dot_general x1, matrix products, per_device(): jnp.dot(normed_all, gate_full, preferred_element_type=jnp.float32)  9.71 us
  transfers between devices with their start and end apart: 8, of which 6 were waited for; matrix products, arithmetic and copies ran while one was open for 6% of the time, Pallas kernels for 0%

profile of v1, /device:TPU:0, one launch (start us, length us, event | category | flops | bytes accessed | tf_op | source)
XLA Modules:
  0.0 391.3 jit_solution(8543122711273827270)
XLA Ops:
  7.4 1.0 fusion.19
  8.4 1.0 fusion.21
  9.4 4.9 %collective-permute-start.1 = (bf16[128,64]{0,1:T(8,128)(2,1)S(1)}, bf16[128,64]{0,1:T(8,128)(2,1)S(1)}, u32[]{:S(2)}, u32[]{:S(2)}) collective-permute-start(bf16[128,64]{0,1:T(8,128)(2,1)S(1)} %slice.18), channel_id=1, source_target_pairs={{0,4},{4,8},{8,12},{12,16},{16,20},{20,24},{24,28},{1,5},{5,9},{9,... | collective-permute-start | bytes 49160 | tf_op jit(solution)/shard_map/ppermute | solution.py:13
  14.3 0.7 slice.14
  15.0 3.4 collective-permute-start
  18.5 1.2 copy.19
  19.6 0.4 reshape.190
  20.3 0.8 multiply_convert_fusion.1
  21.2 0.3 broadcast_and_fusion
  22.0 0.6 fusion.1
  22.8 1.6 copy-done.3
  24.3 0.7 fusion
  25.3 2.8 fusion.12
  28.1 0.3 copy.22
  28.4 2.7 convolution_convert_fusion
  31.2 0.5 all-gather.6.cloned.1.call-update
  31.8 37.5 %reduce-scatter.3.cloned.1.call-done = bf16[768,512]{1,0:T(8,128)(2,1)} async-done(((bf16[768,2048]{1,0:T(8,128)(2,1)}), bf16[768,512]{1,0:T(8,128)(2,1)}) %reduce-scatter.3.cloned.1.call-update) | async-done | bytes 786448 | tf_op jit(solution)/shard_map/reduce_scatter | solution.py:98
  69.2 1.5 fusion.2
  70.7 5.8 %psum.7 = f32[768]{0:T(1024)S(1)} all-reduce(f32[768]{0:T(1024)S(1)} %fusion.2), channel_id=1, replica_groups=mesh['sp'=8,'tp'=4] {'tp'}, use_global_device_ids=true, to_apply=%region_6.7 | all-reduce | flops 768 | bytes 6144 | tf_op jit(solution)/shard_map/psum | solution.py:102
  76.5 2.3 fusion.4
  78.8 2.9 stack.2
  81.7 5.7 %all-to-all-start = ((bf16[8,256,1408]{2,1,0:T(8,128)(2,1)}), bf16[8,256,1408]{2,1,0:T(8,128)(2,1)}, u32[]{:S(2)}, u32[]{:S(2)}) async-start(bf16[8,256,1408]{2,1,0:T(8,128)(2,1)} %stack.2), calls=%async_computation.1 | async-start | bytes 11534336 | tf_op jit(solution)/shard_map/all_to_all | solution.py:48
  87.5 0.5 all-gather.8.cloned.1.call-update
  88.0 0.2 reduce-scatter.5.cloned.1.call-start
  88.3 83.8 %all-gather.6.cloned.1.call-done = bf16[2048,1408]{1,0:T(8,128)(2,1)} async-done(((bf16[256,1408]{1,0:T(8,128)(2,1)}), bf16[2048,1408]{1,0:T(8,128)(2,1)}) %all-gather.6.cloned.1.call-update) | async-done | bytes 5767184 | tf_op jit(solution)/shard_map/all_gather | solution.py:46
  172.1 54.1 %all-gather.4.cloned.1.call-done = bf16[768,2048]{1,0:T(8,128)(2,1)} async-done(((bf16[768,512]{1,0:T(8,128)(2,1)}), bf16[768,2048]{1,0:T(8,128)(2,1)}) %all-gather.4.cloned.1.call-update) | async-done | bytes 3145744 | tf_op jit(solution)/shard_map/all_gather | solution.py:106
  226.2 9.7 %fusion.34 = f32[768,1408]{1,0:T(8,128)} fusion(bf16[768,2048]{1,0:T(8,128)(2,1)} %all-gather.4.cloned.1.call-done, bf16[2048,1408]{1,0:T(8,128)(2,1)} %all-gather.6.cloned.1.call-done), kind=kOutput, calls=%fused_computation.60 | convolution fusion | flops 4429185024 | bytes 13238272 | tf_op jit(solution)/shard_map/dot_general | solution.py:107
  235.9 26.1 %all-to-all-done = bf16[8,256,1408]{2,1,0:T(8,128)(2,1)} async-done(((bf16[8,256,1408]{2,1,0:T(8,128)(2,1)}), bf16[8,256,1408]{2,1,0:T(8,128)(2,1)}, u32[]{:S(2)}, u32[]{:S(2)}) %all-to-all-start) | async-done | bytes 5767200 | tf_op jit(solution)/shard_map/all_to_all | solution.py:48
  262.0 66.4 %all-gather.8.cloned.1.call-done = bf16[1408,2048]{1,0:T(8,128)(2,1)} async-done(((bf16[1408,256]{1,0:T(8,128)(2,1)}), bf16[1408,2048]{1,0:T(8,128)(2,1)}) %all-gather.8.cloned.1.call-update) | async-done | bytes 5767184 | tf_op jit(solution)/shard_map/all_gather | solution.py:51
  328.4 16.9 %convolution_convert_fusion.1 = bf16[768,2048]{1,0:T(8,128)(2,1)} fusion(bf16[1408,2048]{1,0:T(8,128)(2,1)} %all-gather.8.cloned.1.call-done, f32[768,1408]{1,0:T(8,128)} %fusion.34, bf16[768,2048]{1,0:T(8,128)(2,1)} %all-gather.4.cloned.1.call-done, bf16[2048,1408]{1,0:T(8,128)(2,1)} %bitcast.12), kind=kOutput, calls=%fused_computation.2 | convolution fusion | flops 8866430976 | bytes 22151168 | tf_op jit(solution)/shard_map/dot_general | solution.py:110
  345.3 36.1 %reduce-scatter.5.cloned.1.call-done = bf16[768,512]{1,0:T(8,128)(2,1)} async-done(((bf16[768,2048]{1,0:T(8,128)(2,1)}), bf16[768,512]{1,0:T(8,128)(2,1)}) %reduce-scatter.5.cloned.1.call-update) | async-done | bytes 786448 | tf_op jit(solution)/shard_map/reduce_scatter | solution.py:111
  381.4 2.3 fusion.5
  (47 shorter events, 1.3 us)
Async XLA Ops:
  7.4 21.1 %copy-start = (bf16[256,2048]{1,0:T(8,128)(2,1)S(1)}, bf16[256,2048]{1,0:T(8,128)(2,1)}, u32[]{:S(2)}) copy-start(bf16[256,2048]{1,0:T(8,128)(2,1)} %param.18) | copy-start | bytes 3145732
  7.4 14.3 %copy-start.5 = (bf16[768,64]{0,1:T(8,128)(2,1)S(1)}, bf16[768,64]{0,1:T(8,128)(2,1)}, u32[]{:S(2)}) copy-start(bf16[768,64]{0,1:T(8,128)(2,1)} %param.14) | copy-start | bytes 294916
  7.4 61.9 %reduce-scatter.3.cloned.1.call-start = ((), (), s32[]{:S(2)}) async-start(), calls=%async_computation.3 | async-start | bytes 3932160 | tf_op jit(solution)/shard_map/reduce_scatter | solution.py:98
  9.4 12.4 %collective-permute-start.1 = (bf16[128,64]{0,1:T(8,128)(2,1)S(1)}, bf16[128,64]{0,1:T(8,128)(2,1)S(1)}, u32[]{:S(2)}, u32[]{:S(2)}) collective-permute-start(bf16[128,64]{0,1:T(8,128)(2,1)S(1)} %slice.18), channel_id=1, source_target_pairs={{0,4},{4,8},{8,12},{12,16},{16,20},{20,24},{24,28},{1,5},{5,9},{9,... | collective-permute-start | bytes 49160 | tf_op jit(solution)/shard_map/ppermute | solution.py:13
  15.0 10.1 %collective-permute-start = (bf16[128,64]{0,1:T(8,128)(2,1)S(1)}, bf16[128,64]{0,1:T(8,128)(2,1)S(1)}, u32[]{:S(2)}, u32[]{:S(2)}) collective-permute-start(bf16[128,64]{0,1:T(8,128)(2,1)S(1)} %slice.14), channel_id=1, source_target_pairs={{0,4},{4,8},{8,12},{12,16},{16,20},{20,24},{24,28},{1,5},{5,9},{9,... | collective-permute-start | bytes 49160 | tf_op jit(solution)/shard_map/ppermute | solution.py:13
  21.1 1.6 copy-start.6
  22.7 1.6 copy-start.3
  31.1 38.1 %copy-start.1 = (bf16[768,512]{1,0:T(8,128)(2,1)S(1)}, bf16[768,512]{1,0:T(8,128)(2,1)}, u32[]{:S(2)}) copy-start(bf16[768,512]{1,0:T(8,128)(2,1)} %param.19) | copy-start | bytes 2359300
  31.1 45.4 %copy-start.7 = (f32[512]{0:T(512)S(1)}, f32[512]{0:T(512)}, u32[]{:S(2)}) copy-start(f32[512]{0:T(512)} %param.20) | copy-start | bytes 6148
  31.1 47.7 %copy-start.4 = (bf16[256,1408]{1,0:T(8,128)(2,1)S(1)}, bf16[256,1408]{1,0:T(8,128)(2,1)}, u32[]{:S(2)}) copy-start(bf16[256,1408]{1,0:T(8,128)(2,1)} %param.22) | copy-start | bytes 2162692
  31.1 141.0 %all-gather.6.cloned.1.call-start = ((), (), s32[]{:S(2)}) async-start(), calls=%async_computation.5 | async-start | bytes 6488064 | tf_op jit(solution)/shard_map/all_gather | solution.py:46
  31.7 194.5 %all-gather.4.cloned.1.call-start = ((), (), s32[]{:S(2)}) async-start(), calls=%async_computation.4 | async-start | bytes 3932160 | tf_op jit(solution)/shard_map/all_gather | solution.py:106
  81.7 180.3 %all-to-all-start = ((bf16[8,256,1408]{2,1,0:T(8,128)(2,1)}), bf16[8,256,1408]{2,1,0:T(8,128)(2,1)}, u32[]{:S(2)}, u32[]{:S(2)}) async-start(bf16[8,256,1408]{2,1,0:T(8,128)(2,1)} %stack.2), calls=%async_computation.1 | async-start | bytes 11534336 | tf_op jit(solution)/shard_map/all_to_all | solution.py:48
  87.5 241.0 %all-gather.8.cloned.1.call-start = ((), (), s32[]{:S(2)}) async-start(), calls=%async_computation.6 | async-start | bytes 6488064 | tf_op jit(solution)/shard_map/all_gather | solution.py:51
  88.0 293.4 %reduce-scatter.5.cloned.1.call-start = ((), (), s32[]{:S(2)}) async-start(), calls=%async_computation.7 | async-start | bytes 3932160 | tf_op jit(solution)/shard_map/reduce_scatter | solution.py:111
  345.3 36.1 %copy-start.2 = (bf16[768,512]{1,0:T(8,128)(2,1)S(1)}, bf16[768,512]{1,0:T(8,128)(2,1)}, u32[]{:S(2)}) copy-start(bf16[768,512]{1,0:T(8,128)(2,1)} %reduce-scatter.3.cloned.1.call-done) | copy-start | bytes 2359300
Sparse Core Ops, SparseCore 0:
  31.3 37.9 reduce-scatter.2
  345.5 35.8 reduce-scatter.4
Sparse Core Ops, SparseCore 1:
  33.8 138.2 all-gather.5
  173.5 52.6 all-gather.3
  228.1 100.2 all-gather.7
